TPU v7x, 32 devices: a whole 2x2x4 slice. The times are simulated.
32 devices in a mesh: ra: 8 (over z, y), cb: 4 (over x, core).
Axes of the slice: x: 2, y: 2, z: 4, core: 2. Of those that a mesh axis runs over, the one named last changes fastest.
Arguments:
- tokens: bfloat16 [512, 4096], P(None, 'cb'), may hold values from -82 to 82
- gate_weight: float32 [2, 4096, 11264], P(None, 'cb', 'ra'), may hold values from -0.09375 to 0.09375
- up_weight: float32 [2, 4096, 11264], P(None, 'cb', 'ra'), may hold values from -0.09375 to 0.09375
- down_weight: float32 [2, 11264, 4096], P(None, 'ra', 'cb'), may hold values from -0.0546875 to 0.0546875
- gate_scale: float32 [2, 11264], P(None, 'ra'), may hold values from 0.5 to 2
- up_scale: float32 [2, 11264], P(None, 'ra'), may hold values from 0.5 to 2
- down_scale: float32 [2, 4096], P(None, 'cb'), may hold values from 0.5 to 2
- norm_gain: float32 [2, 4096], P(None, 'cb'), may hold values from 0.1 to 1.9
- conv_taps: float32 [2, 3, 11264], P(None, None, 'ra'), may hold values from -3 to 3
- conv_bias: float32 [2, 11264], P(None, 'ra'), may hold values from -3 to 3
Outputs:
- layer_out: bfloat16 [512, 4096], P(None, 'cb')
All inputs are finite; a program needn't handle non-finite values.
Results may differ from a plain program's by a relative error of at most 0.012.
Values may be sent and summed in bfloat16 or wider, within the bound.
A program may use at most 128 MiB of HBM per device.

v0:
```python
import jax
import jax.numpy as jnp
from jax import lax
from jax.sharding import PartitionSpec as P

D = 4096
LAYERS = 2


norm_eps = 1e-06
residual_scale = 0.25


def activate(gate, upward, taps, bias):
    padded = jnp.pad(gate, ((1, 1), (0, 0)))
    mixed = taps[0] * padded[:-2] + taps[1] * padded[1:-1] + taps[2] * padded[2:] + bias
    return (jax.nn.silu(mixed) * upward).astype(jnp.bfloat16)


def per_device(
    tokens,
    gate_weight,
    up_weight,
    down_weight,
    gate_scale,
    up_scale,
    down_scale,
    norm_gain,
    conv_taps,
    conv_bias,
):
    hstate = tokens
    for layer in range(LAYERS):
        wide = hstate.astype(jnp.float32)
        squares_part = jnp.sum(wide * wide, axis=1)
        operand = (wide * norm_gain[layer]).astype(jnp.bfloat16)
        gate_part = jnp.dot(
            operand, gate_weight[layer].astype(jnp.bfloat16), preferred_element_type=jnp.float32
        )
        up_part = jnp.dot(
            operand, up_weight[layer].astype(jnp.bfloat16), preferred_element_type=jnp.float32
        )
        gate_sum, up_sum, square_sum = lax.psum((gate_part, up_part, squares_part), "cb")
        rscale = lax.rsqrt(square_sum / D + norm_eps)[:, None]
        gate = gate_sum * rscale * gate_scale[layer]
        upward = up_sum * rscale * up_scale[layer]
        hidden = activate(gate, upward, conv_taps[layer], conv_bias[layer])
        term = jnp.dot(
            hidden, down_weight[layer].astype(jnp.bfloat16), preferred_element_type=jnp.float32
        )
        branch = lax.psum(term, "ra") * down_scale[layer]
        hstate = (residual_scale * wide + branch).astype(jnp.bfloat16)
    return hstate


def solution(mesh):
    in_specs = (
        P(None, "cb"),
        P(None, "cb", "ra"),
        P(None, "cb", "ra"),
        P(None, "ra", "cb"),
        P(None, "ra"),
        P(None, "ra"),
        P(None, "cb"),
        P(None, "cb"),
        P(None, None, "ra"),
        P(None, "ra"),
    )
    out_specs = P(None, "cb")
    return jax.shard_map(
        per_device, mesh=mesh, in_specs=in_specs, out_specs=out_specs, check_vma=False
    )
```

profile of v0, /device:TPU:0, one launch (start us, length us, event | category | flops | bytes accessed | tf_op | source)
XLA Modules:
  0.0 497.1 jit_solution(6274130120586286872)
XLA Ops:
  6.5 0.8 fusion.24
  7.3 4.9 convert.13
  12.2 9.4 %convert.12 = bf16[2,1024,1408]{2,1,0:T(8,128)(2,1)} convert(f32[2,1024,1408]{2,1,0:T(8,128)} %param.11) | non-fusion elementwise | flops 2883584 | bytes 17301504 | tf_op jit(solution)/shard_map/convert.5
  21.6 3.4 fusion.4
  25.1 3.4 fusion.5
  28.4 0.0 all-reduce.15.cloned.1.call-update
  28.5 0.0 all-reduce.9.cloned.1.call-start
  28.5 7.7 %convert.14 = bf16[2,1408,1024]{2,1,0:T(8,128)(2,1)} convert(f32[2,1408,1024]{2,1,0:T(8,128)} %param.13) | non-fusion elementwise | flops 2883584 | bytes 17301504 | tf_op jit(solution)/shard_map/convert.3
  36.2 0.3 fusion.9
  36.5 9.1 %psum.57 = f32[512]{0:T(512)S(1)} all-reduce(f32[512]{0:T(512)S(1)} %fusion.9), channel_id=1, replica_groups=mesh['ra'=8,'cb'=4] {'cb'}, use_global_device_ids=true, to_apply=%region_2.0 | all-reduce | flops 512 | bytes 4096 | tf_op jit(solution)/shard_map/psum | solution.py:43
  45.7 0.1 slice_reduce_fusion
  45.7 0.1 slice_reduce_fusion.5
  45.8 96.7 %all-reduce.15.cloned.1.call-done = (f32[512,1408]{1,0:T(8,128)}, f32[512,1408]{1,0:T(8,128)}) async-done(((f32[512,1408]{1,0:T(8,128)}, f32[512,1408]{1,0:T(8,128)}), (f32[512,1408]{1,0:T(8,128)}, f32[512,1408]{1,0:T(8,128)})) %all-reduce.15.cloned.1.call-update) | async-done | bytes 5767184 | tf_op jit(solution)/shard_map/psum | solution.py:43
  142.5 2.3 multiply_multiply_fusion.1
  144.8 1.2 copy-done
  146.0 6.1 %fusion.3 = f32[512,1024]{1,0:T(8,128)} fusion(bf16[2,1408,1024]{2,1,0:T(8,128)(2,1)S(1)} %copy-done, f32[512,1408]{1,0:T(8,128)} %get-tuple-element.19, f32[512,1408]{1,0:T(8,128)S(1)} %multiply_multiply_fusion.1, f32[1408]{0:T(1024)S(1)} %get-tuple-element.14, f32[1408]{0:T(1024)S(1)} %get-tuple-element.27, f32[1408]{0:T(1024)S(1)} %get-tuple-element.6, ...), kind=kOutput, calls=%fused_computation.13 | convolution fusion | flops 1486487552 | bytes 10790912 | tf_op jit(solution)/shard_map/dot_general | solution.py:48
  152.1 0.0 all-reduce.9.cloned.1.call-update
  152.1 0.0 all-reduce.13.cloned.1.call-start
  152.2 102.5 %all-reduce.9.cloned.1.call-done = f32[512,1024]{1,0:T(8,128)} async-done(((f32[512,1024]{1,0:T(8,128)}), f32[512,1024]{1,0:T(8,128)}) %all-reduce.9.cloned.1.call-update) | async-done | bytes 2097168 | tf_op jit(solution)/shard_map/psum | solution.py:51
  254.7 2.3 fusion.13
  257.0 5.3 %fusion.2 = f32[512,1408]{1,0:T(8,128)} fusion(bf16[2,1024,1408]{2,1,0:T(8,128)(2,1)} %convert.12, bf16[512,1024]{1,0:T(8,128)(2,1)S(1)} %get-tuple-element.22, f32[1024]{0:T(1024)S(1)} %bitcast.26), kind=kOutput, calls=%fused_computation.11 | convolution fusion | flops 1477967872 | bytes 6819840 | tf_op jit(solution)/shard_map/dot_general | solution.py:37
  262.3 3.5 fusion.1
  265.8 0.0 all-reduce.13.cloned.1.call-update
  265.8 0.0 all-reduce.11.cloned.1.call-start
  265.8 6.3 %psum.61 = f32[512]{0:T(512)S(1)} all-reduce(f32[512]{0:T(512)S(1)} %get-tuple-element.21), channel_id=1, replica_groups=mesh['ra'=8,'cb'=4] {'cb'}, use_global_device_ids=true, to_apply=%region_7.8 | all-reduce | flops 512 | bytes 4096 | tf_op jit(solution)/shard_map/psum | solution.py:43
  272.2 104.1 %all-reduce.13.cloned.1.call-done = (f32[512,1408]{1,0:T(8,128)}, f32[512,1408]{1,0:T(8,128)}) async-done(((f32[512,1408]{1,0:T(8,128)}, f32[512,1408]{1,0:T(8,128)}), (f32[512,1408]{1,0:T(8,128)}, f32[512,1408]{1,0:T(8,128)})) %all-reduce.13.cloned.1.call-update) | async-done | bytes 5767184 | tf_op jit(solution)/shard_map/psum | solution.py:43
  376.3 2.3 multiply_multiply_fusion
  378.6 0.4 copy-done.9
  379.0 6.0 %fusion = f32[512,1024]{1,0:T(8,128)} fusion(bf16[2,1408,1024]{2,1,0:T(8,128)(2,1)} %convert.14, f32[512,1408]{1,0:T(8,128)S(1)} %copy-done.9, f32[512,1408]{1,0:T(8,128)S(1)} %multiply_multiply_fusion, f32[1408]{0:T(1024)S(1)} %get-tuple-element.13, f32[1408]{0:T(1024)S(1)} %get-tuple-element.28, f32[1408]{0:T(1024)S(1)} %get-tuple-element.9, ...), kind=kOutput, calls=%fused_computation.7 | convolution fusion | flops 1486487552 | bytes 10778112 | tf_op jit(solution)/shard_map/dot_general | solution.py:48
  385.0 0.0 all-reduce.11.cloned.1.call-update
  385.0 102.6 %all-reduce.11.cloned.1.call-done = f32[512,1024]{1,0:T(8,128)} async-done(((f32[512,1024]{1,0:T(8,128)}), f32[512,1024]{1,0:T(8,128)}) %all-reduce.11.cloned.1.call-update) | async-done | bytes 2097168 | tf_op jit(solution)/shard_map/psum | solution.py:51
  487.6 2.9 fusion.11
  (28 shorter events, 0.1 us)
Async XLA Ops:
  6.5 136.0 %all-reduce.15.cloned.1.call-start = ((), (), s32[]{:S(2)}) async-start(), calls=%async_computation.3 | async-start | bytes 11534336 | tf_op jit(solution)/shard_map/psum | solution.py:43
  12.2 9.4 %copy-start.1 = (bf16[2,1024,1408]{2,1,0:T(8,128)(2,1)}, bf16[2,1024,1408]{2,1,0:T(8,128)(2,1)S(1)}, u32[]{:S(2)}) copy-start(bf16[2,1024,1408]{2,1,0:T(8,128)(2,1)S(1)} %convert.13) | copy-start | bytes 17301508
  12.2 9.4 %copy-start.3 = (bf16[512,1024]{1,0:T(8,128)(2,1)S(1)}, bf16[512,1024]{1,0:T(8,128)(2,1)}, u32[]{:S(2)}) copy-start(bf16[512,1024]{1,0:T(8,128)(2,1)} %param.10) | copy-start | bytes 3145732
  21.6 3.4 copy-start.2
  28.4 17.2 %copy-start.5 = (f32[2,1408]{1,0:T(2,128)S(1)}, f32[2,1408]{1,0:T(2,128)}, u32[]{:S(2)}) copy-start(f32[2,1408]{1,0:T(2,128)} %param.14) | copy-start | bytes 33796
  28.4 17.2 %copy-start.6 = (f32[2,1408]{1,0:T(2,128)S(1)}, f32[2,1408]{1,0:T(2,128)}, u32[]{:S(2)}) copy-start(f32[2,1408]{1,0:T(2,128)} %param.15) | copy-start | bytes 33796
  28.5 17.2 %copy-start.7 = (f32[2,1408]{1,0:T(2,128)S(1)}, f32[2,1408]{1,0:T(2,128)}, u32[]{:S(2)}) copy-start(f32[2,1408]{1,0:T(2,128)} %param.19) | copy-start | bytes 33796
  28.5 17.3 %copy-start.4 = (f32[2,3,1408]{2,0,1:T(2,128)S(1)}, f32[2,3,1408]{2,0,1:T(2,128)}, u32[]{:S(2)}) copy-start(f32[2,3,1408]{2,0,1:T(2,128)} %param.18) | copy-start | bytes 101380
  28.5 226.3 %all-reduce.9.cloned.1.call-start = ((), (), s32[]{:S(2)}) async-start(), calls=%async_computation | async-start | bytes 4194304 | tf_op jit(solution)/shard_map/psum | solution.py:51
  142.5 3.5 copy-start
  146.0 6.1 %copy-start.8 = (f32[2,1024]{1,0:T(2,128)S(1)}, f32[2,1024]{1,0:T(2,128)}, u32[]{:S(2)}) copy-start(f32[2,1024]{1,0:T(2,128)} %param.16) | copy-start | bytes 24580
  152.1 224.2 %all-reduce.13.cloned.1.call-start = ((), (), s32[]{:S(2)}) async-start(), calls=%async_computation.2 | async-start | bytes 11534336 | tf_op jit(solution)/shard_map/psum | solution.py:43
  254.7 7.6 %slice-start = ((s8[5767168]{0:T(1024)(128)(4,1)}), s8[4194304]{0:T(1024)(128)(4,1)S(1)}, s32[]{:S(2)}) async-start(s8[5767168]{0:T(1024)(128)(4,1)} %bitcast.22), calls=%async_computation.4 | async-start | bytes 8388608
  257.0 5.3 %slice-start.1 = ((s8[5767168]{0:T(1024)(128)(4,1)}), s8[1572864]{0:T(1024)(128)(4,1)S(1)}, s32[]{:S(2)}) async-start(s8[5767168]{0:T(1024)(128)(4,1)} %bitcast.22), calls=%async_computation.5 | async-start | bytes 3145728
  265.8 221.8 %all-reduce.11.cloned.1.call-start = ((), (), s32[]{:S(2)}) async-start(), calls=%async_computation.1 | async-start | bytes 4194304 | tf_op jit(solution)/shard_map/psum | solution.py:51
  376.3 2.7 copy-start.9
Sparse Core Ops, SparseCore 0:
  28.6 113.9 all-reduce.14
  152.2 102.4 all-reduce.8
  265.9 110.3 all-reduce.12
  385.1 102.4 all-reduce.10
where the time goes:
time: 497 us
  waiting for transfers between devices  406 us (82%)
  other arithmetic  31.9 us (6%)
  matrix products  27.6 us (6%)
  blocking collectives  15.4 us (3%)
  between operations  13.3 us (3%)
    psum x2, waiting for transfers between devices, per_device(): branch = lax.psum(term, 'ra') * down_scale[layer]  205 us
    psum x2, waiting for transfers between devices, per_device(): lax.psum((gate_part, up_part, squares_part), 'cb')  201 us
    another operation x3, other arithmetic  21.9 us
    psum x2, blocking collectives, per_device(): lax.psum((gate_part, up_part, squares_part), 'cb')  15.4 us
    dot_general x2, matrix products, per_device(): jnp.dot(hidden, down_weight[layer].astype(jnp.bfloat16), preferred_elemen...  12 us
  transfers between devices with their start and end apart: 4, of which 4 were waited for; matrix products, arithmetic and copies ran while one was open for 2% of the time, Pallas kernels for 0%

commit v1 on v0

v1 whole, which is shorter than its diff:
```python
import functools

import jax
import jax.numpy as jnp
from jax import lax
from jax.experimental import pallas as pl
from jax.experimental.pallas import tpu as pltpu
from jax.sharding import PartitionSpec as P

MESH = pl.DeviceIdType.MESH
norm_eps = 1e-06
residual_scale = 0.25
LANES = 128
LAG = 3


def kernel(
    sizes,
    tok,
    gw_hbm,
    uw_hbm,
    dw_hbm,
    gs,
    us,
    ds_,
    gain,
    taps,
    bias,
    out,
    gw,
    uw,
    dw,
    dwb,
    operand,
    rsb,
    stat,
    part,
    crecv,
    xsend,
    xrecv,
    hid,
    ysend,
    own,
    yrecv,
    zsend,
    zrecv,
    hnew,
    wsem,
    ssem,
    csem,
    xsem,
    hsem,
    ysem,
    zsem,
    asem,
    fsem,
):
    layers, n_tok, d_loc, f_loc, d_all, n_z = sizes
    tiles = f_loc // LANES
    half, quarter = n_tok // 2, n_tok // 4
    zrows = half // n_z
    f32, bf16 = jnp.float32, jnp.bfloat16
    ra, cb = lax.axis_index("ra"), lax.axis_index("cb")
    z, y = ra // 2, ra % 2
    x, c = cb // 2, cb % 2
    core_dev = (ra, x * 2 + (1 - c))
    x_dev = (ra, (1 - x) * 2 + c)
    y_dev = (z * 2 + (1 - y), cb)

    def z_dev(k):
        return (lax.rem(z + k, n_z) * 2 + y, cb)

    def remote(src, dst, sems, dev):
        return pltpu.make_async_remote_copy(
            src_ref=src, dst_ref=dst, send_sem=sems[0], recv_sem=sems[1], device_id=dev, device_id_type=MESH
        )

    def load(l, n):
        src, dst = ((gw_hbm, gw), (uw_hbm, uw), (dw_hbm, dw))[n]
        return pltpu.make_async_copy(src.at[l], dst.at[l], wsem.at[l, n])

    load(0, 0).start()
    load(0, 1).start()

    barrier = pltpu.get_barrier_semaphore()
    peers = [(ra, lax.rem(cb + k, 4)) for k in range(1, 4)] + [y_dev] + [z_dev(k) for k in range(1, n_z)]
    for dev in peers:
        pl.semaphore_signal(barrier, inc=1, device_id=dev, device_id_type=MESH)
    pl.semaphore_wait(barrier, len(peers))

    my_rows = pl.ds(pl.multiple_of(c * half + x * quarter, quarter), quarter)
    x_rows = pl.ds(pl.multiple_of(c * half + (1 - x) * quarter, quarter), quarter)
    peer_half = pl.ds(pl.multiple_of((1 - c) * half, half), half)

    def zr(zz):
        return pl.ds(pl.multiple_of(zz * zrows, zrows), zrows)

    def hr(yy, zz):
        return pl.ds(pl.multiple_of(yy * half + zz * zrows, zrows), zrows)

    for l in range(layers):
        h = tok if l == 0 else hnew.at[l - 1]
        wide = h[...].astype(f32)
        ssq = jnp.sum(wide * wide, axis=1, keepdims=True)
        lane = lax.broadcasted_iota(jnp.int32, (n_tok, LANES), 1)
        row = lax.broadcasted_iota(jnp.int32, (n_tok, LANES), 0)
        pick = lane == lax.shift_right_logical(row, 3)
        packed = jnp.where(pick, jnp.broadcast_to(ssq, (n_tok, LANES)), 0.0)
        stat[l, 0] = jnp.sum(packed.reshape(n_tok // 8, 8, LANES), axis=0)
        for k in range(1, 4):
            remote(
                stat.at[l, 0], stat.at[l, k], (ssem.at[0, l, k - 1], ssem.at[1, l, k - 1]), (ra, lax.rem(cb + k, 4))
            ).start()
        operand[...] = (h[...].astype(f32) * gain[l : l + 1, :]).astype(bf16)
        if l == 0:
            load(0, 0).wait()
            load(0, 1).wait()
            load(0, 2).start()
            for ll in range(1, layers):
                for n in range(3):
                    load(ll, n).start()
        else:
            load(l, 0).wait()
            load(l, 1).wait()
        for k in range(1, 4):
            remote(
                stat.at[l, 0], stat.at[l, k], (ssem.at[0, l, k - 1], ssem.at[1, l, k - 1]), (ra, lax.rem(cb + k, 4))
            ).wait()
        total = stat[l, 0] + stat[l, 1] + stat[l, 2] + stat[l, 3]
        spread = jnp.broadcast_to(total[None], (n_tok // 8, 8, LANES)).reshape(n_tok, LANES)
        summed = jnp.sum(jnp.where(pick, spread, 0.0), axis=1, keepdims=True)
        rsb[...] = jnp.broadcast_to(lax.rsqrt(summed / d_all + norm_eps), (n_tok, LANES))

        def core_copy(j):
            return remote(
                part.at[j, peer_half, :], crecv.at[l, j], (csem.at[0, l, j], csem.at[1, l, j]), core_dev
            )

        def x_copy(j):
            return remote(xsend.at[j], xrecv.at[l, j], (xsem.at[0, l, j], xsem.at[1, l, j]), x_dev)

        x_local = pl.ds(pl.multiple_of((1 - x) * quarter, quarter), quarter)
        m_local = pl.ds(pl.multiple_of(x * quarter, quarter), quarter)

        def gate_step(j, carry):
            @pl.when(j < tiles)
            def _():
                cols = pl.ds(pl.multiple_of(j * LANES, LANES), LANES)
                w = jnp.concatenate([gw[l, :, cols].astype(bf16), uw[l, :, cols].astype(bf16)], axis=1)
                acc = jnp.dot(operand[...], w, preferred_element_type=f32)
                rs = rsb[...]
                g = acc[:, :LANES] * rs * gs[l : l + 1, cols]
                rows = lax.broadcasted_iota(jnp.int32, g.shape, 0)
                prev = jnp.where(rows == 0, 0.0, pltpu.roll(g, 1, 0))
                nxt = jnp.where(rows == n_tok - 1, 0.0, pltpu.roll(g, n_tok - 1, 0))
                mixed = taps[l, 0:1, cols] * prev + taps[l, 1:2, cols] * g + taps[l, 2:3, cols] * nxt
                part[j, :, 0:LANES] = mixed.astype(bf16)
                part[j, :, LANES : 2 * LANES] = (acc[:, LANES:] * rs * us[l : l + 1, cols]).astype(bf16)
                core_copy(j).start()

            @pl.when(j >= LAG)
            def _():
                i = j - LAG
                core_copy(i).wait_recv()
                xsend[i] = (part[i, x_rows, :].astype(f32) + crecv[l, i, x_local, :].astype(f32)).astype(bf16)
                x_copy(i).start()

            return carry

        lax.fori_loop(0, tiles + LAG, gate_step, 0)

        load(l, 2).wait()

        def cast_step(i, carry):
            r = pl.ds(pl.multiple_of(i * LANES, LANES), LANES)
            dwb[r, :] = dw[l, r, :].astype(bf16)
            return carry

        lax.fori_loop(0, tiles, cast_step, 0)

        def h_copy(j, n):
            cols = pl.ds(pl.multiple_of(j * LANES, LANES), LANES)
            block = hid.at[l, x_rows if n == 2 else my_rows, cols]
            return remote(
                block, block, (hsem.at[0, l, n, j], hsem.at[1, l, n, j]), x_dev if n == 0 else core_dev
            )

        def hidden_step(j, carry):
            cols = pl.ds(pl.multiple_of(j * LANES, LANES), LANES)
            x_copy(j).wait_recv()
            s = (
                part[j, my_rows, :].astype(f32)
                + crecv[l, j, m_local, :].astype(f32)
                + xrecv[l, j].astype(f32)
            )
            mixed = s[:, :LANES] + bias[l : l + 1, cols]
            hid[l, my_rows, cols] = (mixed / (1.0 + jnp.exp(-mixed)) * s[:, LANES:]).astype(bf16)
            h_copy(j, 0).start()
            h_copy(j, 1).start()
            return carry

        lax.fori_loop(0, tiles, hidden_step, 0)

        def forward_step(j, carry):
            h_copy(j, 0).wait_recv()
            h_copy(j, 2).start()
            return carry

        lax.fori_loop(0, tiles, forward_step, 0)

        def gathered_step(j, carry):
            h_copy(j, 1).wait_recv()
            h_copy(j, 2).wait_recv()
            core_copy(j).wait_send()
            x_copy(j).wait_send()
            for n in range(3):
                h_copy(j, n).wait_send()
            return carry

        lax.fori_loop(0, tiles, gathered_step, 0)

        def y_copy(k):
            zz = lax.rem(z + k, n_z)
            return remote(
                ysend.at[zr(zz), :], yrecv.at[l, zr(zz), :], (ysem.at[0, l, k - 1], ysem.at[1, l, k - 1]), y_dev
            )

        width = 256
        other_y = pl.ds(pl.multiple_of((1 - y) * half, half), half)
        own_y = pl.ds(pl.multiple_of(y * half, half), half)

        def down_other(i, carry):
            cols = pl.ds(pl.multiple_of(i * width, width), width)
            ysend[:, cols] = jnp.dot(hid[l, other_y, :], dwb[:, cols], preferred_element_type=f32).astype(bf16)
            return carry

        def down_own(i, carry):
            cols = pl.ds(pl.multiple_of(i * width, width), width)
            own[:, cols] = jnp.dot(hid[l, own_y, :], dwb[:, cols], preferred_element_type=f32)
            return carry

        lax.fori_loop(0, d_loc // width, down_other, 0)
        for k in range(1, n_z + 1):
            y_copy(k).start()
        lax.fori_loop(0, d_loc // width, down_own, 0)

        def z_copy(k):
            zz = lax.rem(z + k, n_z)
            return remote(
                zsend.at[zr(zz), :], zrecv.at[l, k - 1], (zsem.at[0, l, k - 1], zsem.at[1, l, k - 1]), z_dev(k)
            )

        for k in range(1, n_z):
            zz = lax.rem(z + k, n_z)
            y_copy(k).wait_recv()
            zsend[zr(zz), :] = (own[zr(zz), :] + yrecv[l, zr(zz), :].astype(f32)).astype(bf16)
            z_copy(k).start()
        y_copy(n_z).wait_recv()
        acc = own[zr(z), :] + yrecv[l, zr(z), :].astype(f32)
        for k in range(1, n_z):
            z_copy(k).wait_recv()
            acc = acc + zrecv[l, k - 1].astype(f32)
        mine = hr(y, z)
        new = residual_scale * h[mine, :].astype(f32) + acc * ds_[l : l + 1, :]
        hnew[l, mine, :] = new.astype(bf16)

        def gather_z(k):
            return remote(
                hnew.at[l, mine, :],
                hnew.at[l, mine, :],
                (asem.at[0, l, k - 1], asem.at[1, l, k - 1]),
                z_dev(k),
            )

        def gather_y(k):
            block = hnew.at[l, hr(y, lax.rem(z + n_z - k, n_z)), :]
            return remote(block, block, (fsem.at[0, l, k], fsem.at[1, l, k]), y_dev)

        for k in range(1, n_z):
            gather_z(k).start()
        gather_y(0).start()
        for k in range(1, n_z):
            gather_z(k).wait_recv()
            gather_y(k).start()
        for k in range(n_z):
            gather_y(k).wait_recv()
        for k in range(1, n_z + 1):
            y_copy(k).wait_send()
        for k in range(1, n_z):
            z_copy(k).wait_send()
            gather_z(k).wait_send()
        for k in range(n_z):
            gather_y(k).wait_send()
    out[...] = hnew[layers - 1]


def fused(n_ra, tokens, gate_weight, up_weight, down_weight, gate_scale, up_scale, down_scale, gain, taps, bias, d_all):
    n_tok, d_loc = tokens.shape
    layers, _, f_loc = gate_weight.shape
    n_z = n_ra // 2
    tiles = f_loc // LANES
    half, quarter = n_tok // 2, n_tok // 4
    f32, bf16 = jnp.float32, jnp.bfloat16
    dma = pltpu.SemaphoreType.DMA
    vmem, hbm = pl.BlockSpec(memory_space=pltpu.VMEM), pl.BlockSpec(memory_space=pl.ANY)
    zrows = half // n_z
    return pl.pallas_call(
        functools.partial(kernel, (layers, n_tok, d_loc, f_loc, d_all, n_z)),
        out_shape=jax.ShapeDtypeStruct((n_tok, d_loc), bf16),
        in_specs=[vmem, hbm, hbm, hbm] + [vmem] * 6,
        out_specs=vmem,
        scratch_shapes=[
            pltpu.VMEM((layers, d_loc, f_loc), f32),
            pltpu.VMEM((layers, d_loc, f_loc), f32),
            pltpu.VMEM((layers, f_loc, d_loc), f32),
            pltpu.VMEM((f_loc, d_loc), bf16),
            pltpu.VMEM((n_tok, d_loc), bf16),
            pltpu.VMEM((n_tok, LANES), f32),
            pltpu.VMEM((layers, 4, 8, LANES), f32),
            pltpu.VMEM((tiles, n_tok, 2 * LANES), bf16),
            pltpu.VMEM((layers, tiles, half, 2 * LANES), bf16),
            pltpu.VMEM((tiles, quarter, 2 * LANES), bf16),
            pltpu.VMEM((layers, tiles, quarter, 2 * LANES), bf16),
            pltpu.VMEM((layers, n_tok, f_loc), bf16),
            pltpu.VMEM((half, d_loc), bf16),
            pltpu.VMEM((half, d_loc), f32),
            pltpu.VMEM((layers, half, d_loc), bf16),
            pltpu.VMEM((half, d_loc), bf16),
            pltpu.VMEM((layers, n_z - 1, zrows, d_loc), bf16),
            pltpu.VMEM((layers, n_tok, d_loc), bf16),
            dma((layers, 3)),
            dma((2, layers, 3)),
            dma((2, layers, tiles)),
            dma((2, layers, tiles)),
            dma((2, layers, 3, tiles)),
            dma((2, layers, n_z)),
            dma((2, layers, n_z - 1)),
            dma((2, layers, n_z - 1)),
            dma((2, layers, n_z)),
        ],
        compiler_params=pltpu.CompilerParams(
            collective_id=0, has_side_effects=True, vmem_limit_bytes=67_043_328
        ),
    )(tokens, gate_weight, up_weight, down_weight, gate_scale, up_scale, down_scale, gain, taps, bias)


def plain(tokens, gate_weight, up_weight, down_weight, gate_scale, up_scale, down_scale, gain, conv_taps, bias, d_all):
    hstate = tokens
    for layer in range(gate_weight.shape[0]):
        wide = hstate.astype(jnp.float32)
        squares = jnp.sum(wide * wide, axis=1)
        operand = (wide * gain[layer]).astype(jnp.bfloat16)
        gate_part = jnp.dot(operand, gate_weight[layer].astype(jnp.bfloat16), preferred_element_type=jnp.float32)
        up_part = jnp.dot(operand, up_weight[layer].astype(jnp.bfloat16), preferred_element_type=jnp.float32)
        gate_sum, up_sum, square_sum = lax.psum((gate_part, up_part, squares), "cb")
        rscale = lax.rsqrt(square_sum / d_all + norm_eps)[:, None]
        gate = gate_sum * rscale * gate_scale[layer]
        upward = up_sum * rscale * up_scale[layer]
        padded = jnp.pad(gate, ((1, 1), (0, 0)))
        taps = conv_taps[layer]
        mixed = taps[0] * padded[:-2] + taps[1] * padded[1:-1] + taps[2] * padded[2:] + bias[layer]
        hidden = (jax.nn.silu(mixed) * upward).astype(jnp.bfloat16)
        term = jnp.dot(hidden, down_weight[layer].astype(jnp.bfloat16), preferred_element_type=jnp.float32)
        branch = lax.psum(term, "ra") * down_scale[layer]
        hstate = (residual_scale * wide + branch).astype(jnp.bfloat16)
    return hstate


def solution(mesh):
    n_ra, n_cb = mesh.shape["ra"], mesh.shape["cb"]

    def per_device(*args):
        n_tok, d_loc = args[0].shape
        f_loc = args[1].shape[2]
        fits = n_cb == 4 and n_ra % 2 == 0 and n_ra >= 4 and n_tok % (16 * n_ra) == 0 and n_tok <= 8 * LANES
        fits = fits and f_loc % LANES == 0 and d_loc % 256 == 0 and f_loc > LAG * LANES
        if fits:
            return fused(n_ra, *args, d_loc * n_cb)
        return plain(*args, d_loc * n_cb)

    in_specs = (
        P(None, "cb"),
        P(None, "cb", "ra"),
        P(None, "cb", "ra"),
        P(None, "ra", "cb"),
        P(None, "ra"),
        P(None, "ra"),
        P(None, "cb"),
        P(None, "cb"),
        P(None, None, "ra"),
        P(None, "ra"),
    )
    return jax.shard_map(
        per_device, mesh=mesh, in_specs=in_specs, out_specs=P(None, "cb"), check_vma=False
    )
```

time: 497 us -> 156 us (0.31)
  waiting for transfers between devices: 406 us -> 0 us
  Pallas kernels: 0 us -> 149 us
  other arithmetic: 31.9 us -> 0 us
  matrix products: 27.6 us -> 0 us
  blocking collectives: 15.4 us -> 0 us
  between operations: 13.3 us -> 0.01 us
    psum x4 -> x0, waiting for transfers between devices: 406 us -> none  [the longest x2 205 us: per_device(): branch = lax.psum(term, 'ra') * down_scale[layer]]
    pallas_call x0 -> x1, Pallas kernels: none -> 149 us  [fused(): pl.pallas_call(functools.partial(kernel, (layers, n_tok, d_loc, f_loc, d_...]
    dot_general x6 -> x0, matrix products: 27.6 us -> none  [the longest x2 12 us: per_device(): jnp.dot(hidden, down_weight[layer].astype(jnp.bfloat16), preferred_elemen...]
    another operation x3 -> x0, other arithmetic: 21.9 us -> none
    psum x2 -> x0, blocking collectives: 15.4 us -> none  [per_device(): lax.psum((gate_part, up_part, squares_part), 'cb')]
  transfers between devices with their start and end apart: 4 -> 0, of which waited for: 4 -> 0; matrix products, arithmetic and copies ran while one was open for 2% -> 0% of each run, Pallas kernels for 0% -> 0%
where the time goes in v1:
time: 156 us; the launch traced here: 153 us
  Pallas kernels  149 us (96%)
  local copies, waits for them, and re-layouts  3.65 us (2%)
    pallas_call x1, Pallas kernels, fused(): pl.pallas_call(functools.partial(kernel, (layers, n_tok, d_loc, f_loc, d_...  149 us
    unnamed x2, local copies, waits for them, and re-layouts  3.65 us

profile of v1, /device:TPU:0, one launch (start us, length us, event | category | flops | bytes accessed | tf_op | source)
XLA Modules:
  0.0 152.7 jit_solution(2582196290366502079)
XLA Ops:
  0.0 1.4 copy.11.taps
  1.4 149.0 %shard_map.100 = bf16[512,1024]{1,0:T(8,128)(2,1)} custom-call(bf16[512,1024]{1,0:T(8,128)(2,1)} %tok.1, f32[2,1024,1408]{2,1,0:T(8,128)} %gw_hbm.1, f32[2,1024,1408]{2,1,0:T(8,128)} %uw_hbm.1, f32[2,1408,1024]{2,1,0:T(8,128)} %dw_hbm.1, f32[2,1408]{1,0:T(2,128)} %gs.1, f32[2,1408]{1,0:T(2,128)} %us.1, f32[2,1024]{1,0:T(2,128)} %ds_.1, f32[2,1024]{1,0:T(2,128)} %gain.1, ...), custom_call_target="tpu_custom_call" | custom-call | tf_op jit(solution)/shard_map/pallas_call | solution.py:307
  150.4 2.3 %copy.13 = bf16[512,1024]{1,0:T(8,128)(2,1)} copy(bf16[512,1024]{1,0:T(8,128)(2,1)} %shard_map.100) | data formatting | bytes 2097152

commit v2 on v1

--- a/solution.py
+++ b/solution.py
@@ -12,6 +12,7 @@
 residual_scale = 0.25
 LANES = 128
 LAG = 3
+CHUNKS = 2
 
 
 def kernel(
@@ -57,7 +58,8 @@
 ):
     layers, n_tok, d_loc, f_loc, d_all, n_z = sizes
     tiles = f_loc // LANES
-    half, quarter = n_tok // 2, n_tok // 4
+    span = n_tok // CHUNKS
+    half, quarter = span // 2, span // 4
     zrows = half // n_z
     f32, bf16 = jnp.float32, jnp.bfloat16
     ra, cb = lax.axis_index("ra"), lax.axis_index("cb")
@@ -88,15 +90,14 @@
         pl.semaphore_signal(barrier, inc=1, device_id=dev, device_id_type=MESH)
     pl.semaphore_wait(barrier, len(peers))
 
-    my_rows = pl.ds(pl.multiple_of(c * half + x * quarter, quarter), quarter)
-    x_rows = pl.ds(pl.multiple_of(c * half + (1 - x) * quarter, quarter), quarter)
-    peer_half = pl.ds(pl.multiple_of((1 - c) * half, half), half)
+    def block_rows(ch, cc, xx):
+        return pl.ds(pl.multiple_of(ch * span + cc * half + xx * quarter, quarter), quarter)
 
     def zr(zz):
         return pl.ds(pl.multiple_of(zz * zrows, zrows), zrows)
 
-    def hr(yy, zz):
-        return pl.ds(pl.multiple_of(yy * half + zz * zrows, zrows), zrows)
+    def hr(ch, yy, zz):
+        return pl.ds(pl.multiple_of(ch * span + yy * half + zz * zrows, zrows), zrows)
 
     for l in range(layers):
         h = tok if l == 0 else hnew.at[l - 1]
@@ -131,16 +132,24 @@
         summed = jnp.sum(jnp.where(pick, spread, 0.0), axis=1, keepdims=True)
         rsb[...] = jnp.broadcast_to(lax.rsqrt(summed / d_all + norm_eps), (n_tok, LANES))
 
-        def core_copy(j):
+        def core_copy(ch, j):
+            rows = pl.ds(pl.multiple_of(ch * span + (1 - c) * half, half), half)
             return remote(
-                part.at[j, peer_half, :], crecv.at[l, j], (csem.at[0, l, j], csem.at[1, l, j]), core_dev
+                part.at[j, rows, :], crecv.at[l, ch, j], (csem.at[0, l, ch, j], csem.at[1, l, ch, j]), core_dev
             )
 
-        def x_copy(j):
-            return remote(xsend.at[j], xrecv.at[l, j], (xsem.at[0, l, j], xsem.at[1, l, j]), x_dev)
+        def x_copy(ch, j):
+            return remote(xsend.at[ch, j], xrecv.at[l, ch, j], (xsem.at[0, l, ch, j], xsem.at[1, l, ch, j]), x_dev)
 
         x_local = pl.ds(pl.multiple_of((1 - x) * quarter, quarter), quarter)
         m_local = pl.ds(pl.multiple_of(x * quarter, quarter), quarter)
+
+        def x_step(ch, i):
+            core_copy(ch, i).wait_recv()
+            xsend[ch, i] = (
+                part[i, block_rows(ch, c, 1 - x), :].astype(f32) + crecv[l, ch, i, x_local, :].astype(f32)
+            ).astype(bf16)
+            x_copy(ch, i).start()
 
         def gate_step(j, carry):
             @pl.when(j < tiles)
@@ -156,14 +165,12 @@
                 mixed = taps[l, 0:1, cols] * prev + taps[l, 1:2, cols] * g + taps[l, 2:3, cols] * nxt
                 part[j, :, 0:LANES] = mixed.astype(bf16)
                 part[j, :, LANES : 2 * LANES] = (acc[:, LANES:] * rs * us[l : l + 1, cols]).astype(bf16)
-                core_copy(j).start()
+                for ch in range(CHUNKS):
+                    core_copy(ch, j).start()
 
             @pl.when(j >= LAG)
             def _():
-                i = j - LAG
-                core_copy(i).wait_recv()
-                xsend[i] = (part[i, x_rows, :].astype(f32) + crecv[l, i, x_local, :].astype(f32)).astype(bf16)
-                x_copy(i).start()
+                x_step(0, j - LAG)
 
             return carry
 
@@ -178,119 +185,158 @@
 
         lax.fori_loop(0, tiles, cast_step, 0)
 
-        def h_copy(j, n):
+        def h_copy(ch, j, n):
             cols = pl.ds(pl.multiple_of(j * LANES, LANES), LANES)
-            block = hid.at[l, x_rows if n == 2 else my_rows, cols]
+            block = hid.at[l, block_rows(ch, c, 1 - x if n == 2 else x), cols]
             return remote(
-                block, block, (hsem.at[0, l, n, j], hsem.at[1, l, n, j]), x_dev if n == 0 else core_dev
+                block, block, (hsem.at[0, l, ch, n, j], hsem.at[1, l, ch, n, j]), x_dev if n == 0 else core_dev
             )
 
-        def hidden_step(j, carry):
-            cols = pl.ds(pl.multiple_of(j * LANES, LANES), LANES)
-            x_copy(j).wait_recv()
-            s = (
-                part[j, my_rows, :].astype(f32)
-                + crecv[l, j, m_local, :].astype(f32)
-                + xrecv[l, j].astype(f32)
-            )
-            mixed = s[:, :LANES] + bias[l : l + 1, cols]
-            hid[l, my_rows, cols] = (mixed / (1.0 + jnp.exp(-mixed)) * s[:, LANES:]).astype(bf16)
-            h_copy(j, 0).start()
-            h_copy(j, 1).start()
-            return carry
-
-        lax.fori_loop(0, tiles, hidden_step, 0)
-
-        def forward_step(j, carry):
-            h_copy(j, 0).wait_recv()
-            h_copy(j, 2).start()
-            return carry
-
-        lax.fori_loop(0, tiles, forward_step, 0)
-
-        def gathered_step(j, carry):
-            h_copy(j, 1).wait_recv()
-            h_copy(j, 2).wait_recv()
-            core_copy(j).wait_send()
-            x_copy(j).wait_send()
-            for n in range(3):
-                h_copy(j, n).wait_send()
-            return carry
-
-        lax.fori_loop(0, tiles, gathered_step, 0)
-
-        def y_copy(k):
+        def hidden(ch):
+            my_rows = block_rows(ch, c, x)
+
+            def step(j, carry):
+                cols = pl.ds(pl.multiple_of(j * LANES, LANES), LANES)
+                x_copy(ch, j).wait_recv()
+                s = (
+                    part[j, my_rows, :].astype(f32)
+                    + crecv[l, ch, j, m_local, :].astype(f32)
+                    + xrecv[l, ch, j].astype(f32)
+                )
+                mixed = s[:, :LANES] + bias[l : l + 1, cols]
+                hid[l, my_rows, cols] = (mixed / (1.0 + jnp.exp(-mixed)) * s[:, LANES:]).astype(bf16)
+                h_copy(ch, j, 0).start()
+                h_copy(ch, j, 1).start()
+                return carry
+
+            lax.fori_loop(0, tiles, step, 0)
+
+        def gather_hidden(ch):
+            def forward_step(j, carry):
+                h_copy(ch, j, 0).wait_recv()
+                h_copy(ch, j, 2).start()
+                return carry
+
+            lax.fori_loop(0, tiles, forward_step, 0)
+
+            def gathered_step(j, carry):
+                h_copy(ch, j, 1).wait_recv()
+                h_copy(ch, j, 2).wait_recv()
+                return carry
+
+            lax.fori_loop(0, tiles, gathered_step, 0)
+
+        def y_copy(ch, k):
             zz = lax.rem(z + k, n_z)
             return remote(
-                ysend.at[zr(zz), :], yrecv.at[l, zr(zz), :], (ysem.at[0, l, k - 1], ysem.at[1, l, k - 1]), y_dev
+                ysend.at[ch, zr(zz), :],
+                yrecv.at[l, ch, zr(zz), :],
+                (ysem.at[0, l, ch, k - 1], ysem.at[1, l, ch, k - 1]),
+                y_dev,
             )
 
-        width = 256
-        other_y = pl.ds(pl.multiple_of((1 - y) * half, half), half)
-        own_y = pl.ds(pl.multiple_of(y * half, half), half)
-
-        def down_other(i, carry):
-            cols = pl.ds(pl.multiple_of(i * width, width), width)
-            ysend[:, cols] = jnp.dot(hid[l, other_y, :], dwb[:, cols], preferred_element_type=f32).astype(bf16)
-            return carry
-
-        def down_own(i, carry):
-            cols = pl.ds(pl.multiple_of(i * width, width), width)
-            own[:, cols] = jnp.dot(hid[l, own_y, :], dwb[:, cols], preferred_element_type=f32)
-            return carry
-
-        lax.fori_loop(0, d_loc // width, down_other, 0)
-        for k in range(1, n_z + 1):
-            y_copy(k).start()
-        lax.fori_loop(0, d_loc // width, down_own, 0)
-
-        def z_copy(k):
+        def down(ch):
+            width = 256
+            other_y = pl.ds(pl.multiple_of(ch * span + (1 - y) * half, half), half)
+            own_y = pl.ds(pl.multiple_of(ch * span + y * half, half), half)
+
+            def down_other(i, carry):
+                cols = pl.ds(pl.multiple_of(i * width, width), width)
+                ysend[ch, :, cols] = jnp.dot(
+                    hid[l, other_y, :], dwb[:, cols], preferred_element_type=f32
+                ).astype(bf16)
+                return carry
+
+            def down_own(i, carry):
+                cols = pl.ds(pl.multiple_of(i * width, width), width)
+                own[ch, :, cols] = jnp.dot(hid[l, own_y, :], dwb[:, cols], preferred_element_type=f32)
+                return carry
+
+            lax.fori_loop(0, d_loc // width, down_other, 0)
+            for k in range(1, n_z + 1):
+                y_copy(ch, k).start()
+            lax.fori_loop(0, d_loc // width, down_own, 0)
+
+        def z_copy(ch, k):
             zz = lax.rem(z + k, n_z)
             return remote(
-                zsend.at[zr(zz), :], zrecv.at[l, k - 1], (zsem.at[0, l, k - 1], zsem.at[1, l, k - 1]), z_dev(k)
-            )
-
-        for k in range(1, n_z):
-            zz = lax.rem(z + k, n_z)
-            y_copy(k).wait_recv()
-            zsend[zr(zz), :] = (own[zr(zz), :] + yrecv[l, zr(zz), :].astype(f32)).astype(bf16)
-            z_copy(k).start()
-        y_copy(n_z).wait_recv()
-        acc = own[zr(z), :] + yrecv[l, zr(z), :].astype(f32)
-        for k in range(1, n_z):
-            z_copy(k).wait_recv()
-            acc = acc + zrecv[l, k - 1].astype(f32)
-        mine = hr(y, z)
-        new = residual_scale * h[mine, :].astype(f32) + acc * ds_[l : l + 1, :]
-        hnew[l, mine, :] = new.astype(bf16)
-
-        def gather_z(k):
-            return remote(
-                hnew.at[l, mine, :],
-                hnew.at[l, mine, :],
-                (asem.at[0, l, k - 1], asem.at[1, l, k - 1]),
+                zsend.at[ch, zr(zz), :],
+                zrecv.at[l, ch, k - 1],
+                (zsem.at[0, l, ch, k - 1], zsem.at[1, l, ch, k - 1]),
                 z_dev(k),
             )
 
-        def gather_y(k):
-            block = hnew.at[l, hr(y, lax.rem(z + n_z - k, n_z)), :]
-            return remote(block, block, (fsem.at[0, l, k], fsem.at[1, l, k]), y_dev)
-
-        for k in range(1, n_z):
-            gather_z(k).start()
-        gather_y(0).start()
-        for k in range(1, n_z):
-            gather_z(k).wait_recv()
-            gather_y(k).start()
-        for k in range(n_z):
-            gather_y(k).wait_recv()
-        for k in range(1, n_z + 1):
-            y_copy(k).wait_send()
-        for k in range(1, n_z):
-            z_copy(k).wait_send()
-            gather_z(k).wait_send()
-        for k in range(n_z):
-            gather_y(k).wait_send()
+        def spread_z(ch):
+            for k in range(1, n_z):
+                zz = lax.rem(z + k, n_z)
+                y_copy(ch, k).wait_recv()
+                zsend[ch, zr(zz), :] = (own[ch, zr(zz), :] + yrecv[l, ch, zr(zz), :].astype(f32)).astype(bf16)
+                z_copy(ch, k).start()
+
+        def gather_z(ch, k):
+            block = hnew.at[l, hr(ch, y, z), :]
+            return remote(block, block, (asem.at[0, l, ch, k - 1], asem.at[1, l, ch, k - 1]), z_dev(k))
+
+        def gather_y(ch, k):
+            block = hnew.at[l, hr(ch, y, lax.rem(z + n_z - k, n_z)), :]
+            return remote(block, block, (fsem.at[0, l, ch, k], fsem.at[1, l, ch, k]), y_dev)
+
+        def finish(ch):
+            y_copy(ch, n_z).wait_recv()
+            acc = own[ch, zr(z), :] + yrecv[l, ch, zr(z), :].astype(f32)
+            for k in range(1, n_z):
+                z_copy(ch, k).wait_recv()
+                acc = acc + zrecv[l, ch, k - 1].astype(f32)
+            mine = hr(ch, y, z)
+            new = residual_scale * h[mine, :].astype(f32) + acc * ds_[l : l + 1, :]
+            hnew[l, mine, :] = new.astype(bf16)
+            for k in range(1, n_z):
+                gather_z(ch, k).start()
+            gather_y(ch, 0).start()
+
+        def forward(ch):
+            for k in range(1, n_z):
+                gather_z(ch, k).wait_recv()
+                gather_y(ch, k).start()
+
+        def second_x(i, carry):
+            x_step(1, i)
+            return carry
+
+        hidden(0)
+        lax.fori_loop(0, tiles, second_x, 0)
+        gather_hidden(0)
+        down(0)
+        spread_z(0)
+        hidden(1)
+        finish(0)
+        gather_hidden(1)
+        down(1)
+        forward(0)
+        spread_z(1)
+        finish(1)
+        forward(1)
+        for ch in range(CHUNKS):
+            for k in range(n_z):
+                gather_y(ch, k).wait_recv()
+
+        for ch in range(CHUNKS):
+
+            def sent_step(j, carry, ch=ch):
+                core_copy(ch, j).wait_send()
+                x_copy(ch, j).wait_send()
+                for n in range(3):
+                    h_copy(ch, j, n).wait_send()
+                return carry
+
+            lax.fori_loop(0, tiles, sent_step, 0)
+            for k in range(1, n_z + 1):
+                y_copy(ch, k).wait_send()
+            for k in range(1, n_z):
+                z_copy(ch, k).wait_send()
+                gather_z(ch, k).wait_send()
+            for k in range(n_z):
+                gather_y(ch, k).wait_send()
     out[...] = hnew[layers - 1]
 
 
@@ -299,7 +345,7 @@
     layers, _, f_loc = gate_weight.shape
     n_z = n_ra // 2
     tiles = f_loc // LANES
-    half, quarter = n_tok // 2, n_tok // 4
+    half, quarter = n_tok // CHUNKS // 2, n_tok // CHUNKS // 4
     f32, bf16 = jnp.float32, jnp.bfloat16
     dma = pltpu.SemaphoreType.DMA
     vmem, hbm = pl.BlockSpec(memory_space=pltpu.VMEM), pl.BlockSpec(memory_space=pl.ANY)
@@ -318,25 +364,25 @@
             pltpu.VMEM((n_tok, LANES), f32),
             pltpu.VMEM((layers, 4, 8, LANES), f32),
             pltpu.VMEM((tiles, n_tok, 2 * LANES), bf16),
-            pltpu.VMEM((layers, tiles, half, 2 * LANES), bf16),
-            pltpu.VMEM((tiles, quarter, 2 * LANES), bf16),
-            pltpu.VMEM((layers, tiles, quarter, 2 * LANES), bf16),
+            pltpu.VMEM((layers, CHUNKS, tiles, half, 2 * LANES), bf16),
+            pltpu.VMEM((CHUNKS, tiles, quarter, 2 * LANES), bf16),
+            pltpu.VMEM((layers, CHUNKS, tiles, quarter, 2 * LANES), bf16),
             pltpu.VMEM((layers, n_tok, f_loc), bf16),
-            pltpu.VMEM((half, d_loc), bf16),
-            pltpu.VMEM((half, d_loc), f32),
-            pltpu.VMEM((layers, half, d_loc), bf16),
-            pltpu.VMEM((half, d_loc), bf16),
-            pltpu.VMEM((layers, n_z - 1, zrows, d_loc), bf16),
+            pltpu.VMEM((CHUNKS, half, d_loc), bf16),
+            pltpu.VMEM((CHUNKS, half, d_loc), f32),
+            pltpu.VMEM((layers, CHUNKS, half, d_loc), bf16),
+            pltpu.VMEM((CHUNKS, half, d_loc), bf16),
+            pltpu.VMEM((layers, CHUNKS, n_z - 1, zrows, d_loc), bf16),
             pltpu.VMEM((layers, n_tok, d_loc), bf16),
             dma((layers, 3)),
             dma((2, layers, 3)),
-            dma((2, layers, tiles)),
-            dma((2, layers, tiles)),
-            dma((2, layers, 3, tiles)),
-            dma((2, layers, n_z)),
-            dma((2, layers, n_z - 1)),
-            dma((2, layers, n_z - 1)),
-            dma((2, layers, n_z)),
+            dma((2, layers, CHUNKS, tiles)),
+            dma((2, layers, CHUNKS, tiles)),
+            dma((2, layers, CHUNKS, 3, tiles)),
+            dma((2, layers, CHUNKS, n_z)),
+            dma((2, layers, CHUNKS, n_z - 1)),
+            dma((2, layers, CHUNKS, n_z - 1)),
+            dma((2, layers, CHUNKS, n_z)),
         ],
         compiler_params=pltpu.CompilerParams(
             collective_id=0, has_side_effects=True, vmem_limit_bytes=67_043_328
@@ -372,7 +418,7 @@
     def per_device(*args):
         n_tok, d_loc = args[0].shape
         f_loc = args[1].shape[2]
-        fits = n_cb == 4 and n_ra % 2 == 0 and n_ra >= 4 and n_tok % (16 * n_ra) == 0 and n_tok <= 8 * LANES
+        fits = n_cb == 4 and n_ra % 2 == 0 and n_ra >= 4 and n_tok % (16 * CHUNKS * n_ra) == 0 and n_tok <= 8 * LANES
         fits = fits and f_loc % LANES == 0 and d_loc % 256 == 0 and f_loc > LAG * LANES
         if fits:
             return fused(n_ra, *args, d_loc * n_cb)

time: 156 us -> 134 us (0.86); the launches traced: 153 us -> 133 us
  Pallas kernels: 149 us -> 130 us
    pallas_call x1, Pallas kernels: 149 us -> 130 us  [fused(): pl.pallas_call(functools.partial(kernel, (layers, n_tok, d_loc, f_loc, d_...]
where the time goes in v2:
time: 134 us; the launch traced here: 133 us
  Pallas kernels  130 us (97%)
  local copies, waits for them, and re-layouts  3.65 us (3%)
    pallas_call x1, Pallas kernels, fused(): pl.pallas_call(functools.partial(kernel, (layers, n_tok, d_loc, f_loc, d_...  130 us
    unnamed x2, local copies, waits for them, and re-layouts  3.65 us

profile of v2, /device:TPU:0, one launch (start us, length us, event | category | flops | bytes accessed | tf_op | source)
XLA Modules:
  0.0 133.3 jit_solution(3809554125032544110)
XLA Ops:
  0.0 1.4 %copy.11.taps = f32[2,3,1408]{2,1,0:T(4,128)} copy(f32[2,3,1408]{2,0,1:T(2,128)} %param.18) | data formatting | bytes 67584 | tf_op args[8]
  1.4 129.7 %shard_map.100 = bf16[512,1024]{1,0:T(8,128)(2,1)} custom-call(bf16[512,1024]{1,0:T(8,128)(2,1)} %tok.1, f32[2,1024,1408]{2,1,0:T(8,128)} %gw_hbm.1, f32[2,1024,1408]{2,1,0:T(8,128)} %uw_hbm.1, f32[2,1408,1024]{2,1,0:T(8,128)} %dw_hbm.1, f32[2,1408]{1,0:T(2,128)} %gs.1, f32[2,1408]{1,0:T(2,128)} %us.1, f32[2,1024]{1,0:T(2,128)} %ds_.1, f32[2,1024]{1,0:T(2,128)} %gain.1, ...), custom_call_target="tpu_custom_call" | custom-call | tf_op jit(solution)/shard_map/pallas_call | solution.py:353
  131.1 2.3 %copy.13 = bf16[512,1024]{1,0:T(8,128)(2,1)} copy(bf16[512,1024]{1,0:T(8,128)(2,1)} %shard_map.100) | data formatting | bytes 2097152
